TPU v7x, 32 devices: a whole 2x2x4 slice. The times are simulated.
32 devices in a mesh: grp: 2 (over x), sp: 4 (over y, core), tp: 4 (over z).
Axes of the slice: x: 2, y: 2, z: 4, core: 2. Of those that a mesh axis runs over, the one named last changes fastest.
Arguments:
- tokens_in: bfloat16 [2048, 2048], P(('grp', 'sp'), 'tp'), parts along dimension 0, may hold values from -8 to 8
- out_gate: bfloat16 [3, 2048, 2048], P(None, 'sp', 'tp'), may hold values from -0.125 to 0.125
- in_gate: bfloat16 [3, 2048, 2048], P(None, 'sp', 'tp'), may hold values from -0.125 to 0.125
- value_proj: bfloat16 [3, 2048, 2048], P(None, 'sp', 'tp'), may hold values from -0.125 to 0.125
- mix_proj: bfloat16 [3, 2048, 2048], P(None, 'sp', 'tp'), may hold values from -0.125 to 0.125
- conv_taps: float32 [3, 3, 2048], P(None, None, 'tp'), may hold values from -3.5 to 3.5
- norm_gains: float32 [3, 2048], P(None, 'tp'), may hold values from 0.1 to 1.9
- final_gain: float32 [2048], P('tp'), may hold values from 0.1 to 1.9
Outputs:
- normed_out: bfloat16 [2048, 2048], P(('grp', 'sp'), 'tp'), parts along dimension 0
There are 2 independent parts, one for each index of `grp`. A program takes and returns all parts, laid end to end along the dimension named above; an argument that names none is the same for every part. Nothing has to cross between parts.
All inputs are finite; a program needn't handle non-finite values.
Results may differ from a plain program's by a relative error of at most 0.025.
Values may be sent and summed in bfloat16 or wider, within the bound.
A program may use at most 64 MiB of HBM per device.

v0:
```python
import jax
import jax.numpy as jnp
from jax import lax
from jax.sharding import PartitionSpec as P

D = 2048
TAPS = 3
LAYERS = 3


epsilon = 1e-06


def passed_along(shard, axis, by):
    peers = lax.axis_size(axis)
    pairs = [(i, i + by) for i in range(peers) if 0 <= i + by < peers]
    return lax.ppermute(shard, axis, pairs)


def row_scale(stream):
    squares = lax.psum(jnp.sum(stream * stream, axis=1, keepdims=True), "tp")
    return lax.rsqrt(squares / D + epsilon)


def shards(tokens_in, out_gate, in_gate, value_proj, mix_proj, conv_taps, norm_gains, final_gain):
    stream = tokens_in.astype(jnp.float32)
    row_count = stream.shape[0]
    reach = TAPS - 1
    whole = (
        lax.all_gather(out_gate, "sp", axis=1, tiled=True),
        lax.all_gather(in_gate, "sp", axis=1, tiled=True),
        lax.all_gather(value_proj, "sp", axis=1, tiled=True),
        lax.all_gather(mix_proj, "sp", axis=1, tiled=True),
    )
    for layer_index in range(LAYERS):
        scale = row_scale(stream)
        normed = (stream * norm_gains[layer_index]).astype(jnp.bfloat16)
        gathered = lax.all_gather(normed, "tp", axis=1, tiled=True)
        products = tuple(
            (
                jnp.dot(gathered, weight[layer_index], preferred_element_type=jnp.float32)
                for weight in whole[:3]
            )
        )
        out_gates, in_gates, values = [
            (product * scale).astype(jnp.bfloat16) for product in products
        ]
        product_v = (in_gates.astype(jnp.float32) * values.astype(jnp.float32)).astype(jnp.bfloat16)
        earlier = passed_along(product_v[row_count - reach :], "sp", 1)
        padded = jnp.concatenate([earlier, product_v], axis=0)
        convolved = padded[0:row_count].astype(jnp.float32) * conv_taps[layer_index, 0]
        for tap_index in range(1, TAPS):
            convolved = (
                convolved
                + padded[tap_index : tap_index + row_count].astype(jnp.float32)
                * conv_taps[layer_index, tap_index]
            )
        gated = (out_gates.astype(jnp.float32) * convolved).astype(jnp.bfloat16)
        spread = lax.all_gather(gated, "tp", axis=1, tiled=True)
        mixed = jnp.dot(spread, whole[3][layer_index], preferred_element_type=jnp.float32)
        stream = stream + mixed
    scale = row_scale(stream)
    return (stream * scale * final_gain).astype(jnp.bfloat16)


def solution(mesh):
    in_specs = (
        P(("grp", "sp"), "tp"),
        P(None, "sp", "tp"),
        P(None, "sp", "tp"),
        P(None, "sp", "tp"),
        P(None, "sp", "tp"),
        P(None, None, "tp"),
        P(None, "tp"),
        P("tp"),
    )
    out_specs = P(("grp", "sp"), "tp")
    return jax.shard_map(shards, mesh=mesh, in_specs=in_specs, out_specs=out_specs, check_vma=False)
```

profile of v0, /device:TPU:0, one launch (start us, length us, event | category | flops | bytes accessed | tf_op | source)
XLA Modules:
  0.0 424.5 jit_solution(9574232206159354128)
XLA Ops:
  11.8 13.5 %psum.28 = f32[256,1]{0,1:T(1,128)S(1)} all-reduce(f32[256,1]{0,1:T(1,128)S(1)} %bitcast.159), channel_id=1, replica_groups=mesh['grp'=2,'sp'=4,'tp'=4] {'tp'}, use_global_device_ids=true, to_apply=%region_1.0 | all-reduce | flops 256 | bytes 2048 | tf_op jit(solution)/shard_map/psum | solution.py:21
  25.3 14.7 %all-gather.11.cloned.1.call-done = bf16[256,2048]{1,0:T(8,128)(2,1)} async-done(((bf16[256,512]{1,0:T(8,128)(2,1)}), bf16[256,2048]{1,0:T(8,128)(2,1)}) %all-gather.11.cloned.1.call-update) | async-done | bytes 1048592 | tf_op jit(solution)/shard_map/all_gather | solution.py:38
  40.0 47.3 %all-gather.17.cloned.1.call-done = bf16[3,2048,512]{2,1,0:T(8,128)(2,1)} async-done(((bf16[3,512,512]{2,1,0:T(8,128)(2,1)}), bf16[3,2048,512]{2,1,0:T(8,128)(2,1)}) %all-gather.17.cloned.1.call-update) | async-done | bytes 6291472 | tf_op jit(solution)/shard_map/all_gather | solution.py:32
  90.0 45.3 %all-gather.15.cloned.1.call-done = bf16[3,2048,512]{2,1,0:T(8,128)(2,1)} async-done(((bf16[3,512,512]{2,1,0:T(8,128)(2,1)}), bf16[3,2048,512]{2,1,0:T(8,128)(2,1)}) %all-gather.15.cloned.1.call-update) | async-done | bytes 6291472 | tf_op jit(solution)/shard_map/all_gather | solution.py:31
  140.1 43.0 %all-gather.13.cloned.1.call-done = bf16[3,2048,512]{2,1,0:T(8,128)(2,1)} async-done(((bf16[3,512,512]{2,1,0:T(8,128)(2,1)}), bf16[3,2048,512]{2,1,0:T(8,128)(2,1)}) %all-gather.13.cloned.1.call-update) | async-done | bytes 6291472 | tf_op jit(solution)/shard_map/all_gather | solution.py:30
  183.1 3.1 fusion.35
  186.3 44.6 %all-gather.21.cloned.1.call-done = bf16[3,2048,512]{2,1,0:T(8,128)(2,1)} async-done(((bf16[3,512,512]{2,1,0:T(8,128)(2,1)}), bf16[3,2048,512]{2,1,0:T(8,128)(2,1)}) %all-gather.21.cloned.1.call-update) | async-done | bytes 6291472 | tf_op jit(solution)/shard_map/all_gather | solution.py:33
  230.9 29.4 %all-gather.19.cloned.1.call-done = bf16[256,2048]{1,0:T(8,128)(2,1)} async-done(((bf16[256,512]{1,0:T(8,128)(2,1)}), bf16[256,2048]{1,0:T(8,128)(2,1)}) %all-gather.19.cloned.1.call-update) | async-done | bytes 1048592 | tf_op jit(solution)/shard_map/all_gather | solution.py:59
  260.3 3.4 multiply_reduce_fusion.2
  263.8 10.3 %psum.29 = f32[256,1]{0,1:T(1,128)S(1)} all-reduce(f32[256,1]{0,1:T(1,128)S(1)} %bitcast.182), channel_id=1, replica_groups=mesh['grp'=2,'sp'=4,'tp'=4] {'tp'}, use_global_device_ids=true, to_apply=%region_3.0 | all-reduce | flops 256 | bytes 2048 | tf_op jit(solution)/shard_map/psum | solution.py:21
  274.1 17.2 %all-gather.23.cloned.1.call-done = bf16[256,2048]{1,0:T(8,128)(2,1)} async-done(((bf16[256,512]{1,0:T(8,128)(2,1)}), bf16[256,2048]{1,0:T(8,128)(2,1)}) %all-gather.23.cloned.1.call-update) | async-done | bytes 1048592 | tf_op jit(solution)/shard_map/all_gather | solution.py:38
  291.2 2.7 fusion.46
  293.9 2.6 fusion.45
  298.7 3.1 fusion.42
  301.9 30.3 %all-gather.25.cloned.1.call-done = bf16[256,2048]{1,0:T(8,128)(2,1)} async-done(((bf16[256,512]{1,0:T(8,128)(2,1)}), bf16[256,2048]{1,0:T(8,128)(2,1)}) %all-gather.25.cloned.1.call-update) | async-done | bytes 1048592 | tf_op jit(solution)/shard_map/all_gather | solution.py:59
  332.2 3.3 multiply_reduce_fusion.1
  335.6 10.3 %psum.30 = f32[256,1]{0,1:T(1,128)S(1)} all-reduce(f32[256,1]{0,1:T(1,128)S(1)} %bitcast.181), channel_id=1, replica_groups=mesh['grp'=2,'sp'=4,'tp'=4] {'tp'}, use_global_device_ids=true, to_apply=%region_5.0 | all-reduce | flops 256 | bytes 2048 | tf_op jit(solution)/shard_map/psum | solution.py:21
  345.9 17.2 %all-gather.27.cloned.1.call-done = bf16[256,2048]{1,0:T(8,128)(2,1)} async-done(((bf16[256,512]{1,0:T(8,128)(2,1)}), bf16[256,2048]{1,0:T(8,128)(2,1)}) %all-gather.27.cloned.1.call-update) | async-done | bytes 1048592 | tf_op jit(solution)/shard_map/all_gather | solution.py:38
  363.0 2.7 fusion.53
  365.7 2.6 fusion.52
  370.5 3.1 fusion.49
  373.6 30.3 %all-gather.29.cloned.1.call-done = bf16[256,2048]{1,0:T(8,128)(2,1)} async-done(((bf16[256,512]{1,0:T(8,128)(2,1)}), bf16[256,2048]{1,0:T(8,128)(2,1)}) %all-gather.29.cloned.1.call-update) | async-done | bytes 1048592 | tf_op jit(solution)/shard_map/all_gather | solution.py:59
  404.0 2.7 multiply_reduce_fusion
  406.7 10.2 %psum.31 = f32[256,1]{0,1:T(1,128)S(1)} all-reduce(f32[256,1]{0,1:T(1,128)S(1)} %bitcast.183), channel_id=1, replica_groups=mesh['grp'=2,'sp'=4,'tp'=4] {'tp'}, use_global_device_ids=true, to_apply=%region_7.0 | all-reduce | flops 256 | bytes 2048 | tf_op jit(solution)/shard_map/psum | solution.py:21
  (51 shorter events, 17.9 us)
Async XLA Ops:
  6.5 33.5 %all-gather.11.cloned.1.call-start = ((), (), s32[]{:S(2)}) async-start(), calls=%async_computation | async-start | bytes 1310720 | tf_op jit(solution)/shard_map/all_gather | solution.py:38
  9.1 78.2 %all-gather.17.cloned.1.call-start = ((), (), s32[]{:S(2)}) async-start(), calls=%async_computation.3 | async-start | bytes 7864320 | tf_op jit(solution)/shard_map/all_gather | solution.py:32
  9.9 125.4 %all-gather.15.cloned.1.call-start = ((), (), s32[]{:S(2)}) async-start(), calls=%async_computation.2 | async-start | bytes 7864320 | tf_op jit(solution)/shard_map/all_gather | solution.py:31
  10.6 129.5 %copy-start.1 = (f32[3,3,512]{2,1,0:T(4,128)S(1)}, f32[3,3,512]{2,1,0:T(4,128)}, u32[]{:S(2)}) copy-start(f32[3,3,512]{2,1,0:T(4,128)} %param.13) | copy-start | bytes 55300
  10.6 172.5 %all-gather.13.cloned.1.call-start = ((), (), s32[]{:S(2)}) async-start(), calls=%async_computation.1 | async-start | bytes 7864320 | tf_op jit(solution)/shard_map/all_gather | solution.py:30
  11.2 219.7 %all-gather.21.cloned.1.call-start = ((), (), s32[]{:S(2)}) async-start(), calls=%async_computation.5 | async-start | bytes 7864320 | tf_op jit(solution)/shard_map/all_gather | solution.py:33
  11.8 248.6 %all-gather.19.cloned.1.call-start = ((), (), s32[]{:S(2)}) async-start(), calls=%async_computation.4 | async-start | bytes 1310720 | tf_op jit(solution)/shard_map/all_gather | solution.py:59
  40.0 143.1 %copy-start.3 = (bf16[256,2048]{1,0:T(8,128)(2,1)S(1)}, bf16[256,2048]{1,0:T(8,128)(2,1)}, u32[]{:S(2)}) copy-start(bf16[256,2048]{1,0:T(8,128)(2,1)} %all-gather.11.cloned.1.call-done) | copy-start | bytes 3145732
  90.0 170.4 %copy-start = (bf16[256,512]{1,0:T(8,128)(2,1)S(1)}, bf16[256,512]{1,0:T(8,128)(2,1)}, u32[]{:S(2)}) copy-start(bf16[256,512]{1,0:T(8,128)(2,1)} %param.8) | copy-start | bytes 786436
  137.9 45.2 %collective-permute-start = (bf16[2,512]{1,0:T(2,128)(2,1)S(1)}, bf16[2,512]{1,0:T(2,128)(2,1)S(1)}, u32[]{:S(2)}, u32[]{:S(2)}) collective-permute-start(bf16[2,512]{1,0:T(2,128)(2,1)S(1)} %slice.135), channel_id=1, source_target_pairs={{0,4},{4,8},{8,12},{1,5},{5,9},{9,13},{2,6},{6,10},{10,14},{3,7},{... | collective-permute-start | bytes 6152 | tf_op jit(solution)/shard_map/ppermute | solution.py:17
  186.2 105.0 %all-gather.23.cloned.1.call-start = ((), (), s32[]{:S(2)}) async-start(), calls=%async_computation.6 | async-start | bytes 1310720 | tf_op jit(solution)/shard_map/all_gather | solution.py:38
  263.7 68.4 %all-gather.25.cloned.1.call-start = ((), (), s32[]{:S(2)}) async-start(), calls=%async_computation.7 | async-start | bytes 1310720 | tf_op jit(solution)/shard_map/all_gather | solution.py:59
  291.2 7.5 %copy-start.5 = (bf16[256,2048]{1,0:T(8,128)(2,1)S(1)}, bf16[256,2048]{1,0:T(8,128)(2,1)}, u32[]{:S(2)}) copy-start(bf16[256,2048]{1,0:T(8,128)(2,1)} %all-gather.23.cloned.1.call-done) | copy-start | bytes 3145732
  296.6 2.1 collective-permute-start.1
  301.8 61.2 %all-gather.27.cloned.1.call-start = ((), (), s32[]{:S(2)}) async-start(), calls=%async_computation.8 | async-start | bytes 1310720 | tf_op jit(solution)/shard_map/all_gather | solution.py:38
  335.5 68.4 %all-gather.29.cloned.1.call-start = ((), (), s32[]{:S(2)}) async-start(), calls=%async_computation.9 | async-start | bytes 1310720 | tf_op jit(solution)/shard_map/all_gather | solution.py:59
  363.0 7.5 %copy-start.4 = (bf16[256,2048]{1,0:T(8,128)(2,1)S(1)}, bf16[256,2048]{1,0:T(8,128)(2,1)}, u32[]{:S(2)}) copy-start(bf16[256,2048]{1,0:T(8,128)(2,1)} %all-gather.27.cloned.1.call-done) | copy-start | bytes 3145732
  368.4 48.5 %copy-start.2 = (f32[512]{0:T(512)S(1)}, f32[512]{0:T(512)}, u32[]{:S(2)}) copy-start(f32[512]{0:T(512)} %param.15) | copy-start | bytes 6148
  368.4 2.1 collective-permute-start.2
Sparse Core Ops, SparseCore 0:
  9.2 30.7 all-gather.10
  41.6 45.7 all-gather.16
  88.9 46.3 all-gather.14
  136.7 46.3 all-gather.12
  184.5 46.3 all-gather.20
  232.3 27.9 all-gather.18
  263.8 27.3 all-gather.22
  302.0 30.1 all-gather.24
  335.6 27.3 all-gather.26
  373.8 30.1 all-gather.28
where the time goes:
time: 425 us
  waiting for transfers between devices  323 us (76%)
  blocking collectives  44.2 us (10%)
  matrix products  34.6 us (8%)
  between operations  13.7 us (3%)
  starting transfers between devices  5.1 us (1%)
    all_gather x3, waiting for transfers between devices, shards(): spread = lax.all_gather(gated, 'tp', axis=1, tiled=True)  90 us
    all_gather x3, waiting for transfers between devices, shards(): gathered = lax.all_gather(normed, 'tp', axis=1, tiled=True)  49.1 us
    all_gather x1, waiting for transfers between devices, shards(): lax.all_gather(value_proj, 'sp', axis=1, tiled=True)  47.3 us
    all_gather x1, waiting for transfers between devices, shards(): lax.all_gather(in_gate, 'sp', axis=1, tiled=True)  45.3 us
    all_gather x1, waiting for transfers between devices, shards(): lax.all_gather(mix_proj, 'sp', axis=1, tiled=True)  44.6 us
    psum x4, blocking collectives, row_scale(): squares = lax.psum(jnp.sum(stream * stream, axis=1, keepdims=True), 'tp')  44.2 us
    all_gather x1, waiting for transfers between devices, shards(): lax.all_gather(out_gate, 'sp', axis=1, tiled=True)  43 us
    dot_general x9, matrix products, shards(): jnp.dot(gathered, weight[layer_index], preferred_element_type=jnp.float32)  25.2 us
  transfers between devices with their start and end apart: 13, of which 12 were waited for; matrix products, arithmetic and copies ran while one was open for 2% of the time, Pallas kernels for 0%

commit v1 on v0

v1 whole, which is shorter than its diff:
```python
import functools

import jax
import jax.numpy as jnp
from jax import lax
from jax.experimental import pallas as pl
from jax.experimental.pallas import tpu as pltpu
from jax.sharding import PartitionSpec as P

epsilon = 1e-06
MESH = pl.DeviceIdType.MESH
HALO = 16
CORES = 2
VMEM_LIMIT = 67043328


def kernel(
    sizes,
    tokens,
    in_gate,
    value_proj,
    out_gate,
    mix_proj,
    taps,
    gains,
    final_gain,
    out,
    weights,
    gather_a,
    gather_b,
    squares_a,
    squares_b,
    stream,
    products,
    halo,
    own_sem,
    halo_sems,
    pair_send,
    pair_recv,
    row_send,
    row_recv,
    cross_send,
    cross_recv,
    relay_send,
    relay_recv,
    act_send,
    act_recv,
    act_fwd,
    sq_send,
    sq_recv,
):
    groups, sp_count, tp_count, layers, tap_count = sizes
    rows, width = tokens.shape
    depth = in_gate.shape[1]
    full = depth * sp_count
    part = depth // groups
    chips = sp_count // CORES
    mats = (in_gate, value_proj, out_gate, mix_proj)
    g = lax.axis_index("grp")
    s = lax.axis_index("sp")
    t = lax.axis_index("tp")
    y, core = s // CORES, s % CORES
    partner = y * CORES + (1 - core)
    half = rows // 2
    counts = (HALO + half, rows - half)
    starts = (0, HALO + half)
    gathers = (gather_a, gather_b)
    squares = (squares_a, squares_b)

    def remote(src, dst, send, recv, where):
        return pltpu.make_async_remote_copy(
            src_ref=src, dst_ref=dst, send_sem=send, recv_sem=recv, device_id=where, device_id_type=MESH
        )

    barrier = pltpu.get_barrier_semaphore()
    for axis, me, count in (("tp", t, tp_count), ("sp", s, sp_count), ("grp", g, groups)):
        for by in range(1, count):
            pl.semaphore_signal(barrier, inc=1, device_id={axis: lax.rem(me + by, count)}, device_id_type=MESH)

    for c in range(2):
        for index in range(layers + 1):
            squares[c][index, t] = jnp.zeros(squares[c].shape[2:], jnp.float32)
    products[0:8, :] = jnp.zeros((8, width), jnp.float32)

    @pl.when(s == 0)
    def _():
        halo[...] = jnp.zeros_like(halo)

    pl.semaphore_wait(barrier, tp_count - 1 + sp_count - 1 + groups - 1)

    def block(index, owner, piece):
        return weights.at[index, pl.ds(pl.multiple_of(owner * depth + piece * part, 8), part), :]

    def whole_block(index, owner):
        return weights.at[index, pl.ds(pl.multiple_of(owner * depth, 8), depth), :]

    def own_copy(layer, m):
        index = layer * 4 + m
        return pltpu.make_async_copy(mats[m].at[layer], whole_block(index, s), own_sem.at[index])

    def pair_copy(layer, m, owner):
        index = layer * 4 + m
        return remote(
            mats[m].at[layer], whole_block(index, owner), pair_send.at[index], pair_recv.at[index], {"sp": partner}
        )

    def row_copy(layer, m, by):
        index = layer * 4 + m
        to = lax.rem(y + by, chips) * CORES + core
        return remote(
            mats[m].at[layer, pl.ds(pl.multiple_of(g * part, 8), part), :],
            block(index, s, g),
            row_send.at[index, by - 1],
            row_recv.at[index, by - 1],
            {"sp": to},
        )

    def source(by):
        return lax.rem(y + chips - by, chips) * CORES + core

    def row_arrival(index, by):
        ref = block(index, source(by), g)
        return remote(ref, ref, row_send.at[index, by - 1], row_recv.at[index, by - 1], {"sp": partner})

    def cross_copy(index, by, step):
        ref = block(index, source(by), g)
        return remote(
            ref,
            ref,
            cross_send.at[index, by - 1, step - 1],
            cross_recv.at[index, by - 1, step - 1],
            {"grp": lax.rem(g + step, groups)},
        )

    def cross_arrival(index, by, step):
        ref = block(index, source(by), lax.rem(g + groups - step, groups))
        return remote(
            ref,
            ref,
            cross_send.at[index, by - 1, step - 1],
            cross_recv.at[index, by - 1, step - 1],
            {"grp": lax.rem(g + step, groups)},
        )

    def relay_copy(index, by, step, of_partner=False):
        owner = source(by)
        if of_partner:
            owner = lax.rem(y + chips - by, chips) * CORES + (1 - core)
        ref = block(index, owner, lax.rem(g + groups - step, groups))
        return remote(
            ref, ref, relay_send.at[index, by - 1, step], relay_recv.at[index, by - 1, step], {"sp": partner}
        )

    def serve_rows(index):
        for by in range(1, chips):
            row_arrival(index, by).wait_recv()
            for step in range(1, groups):
                cross_copy(index, by, step).start()
            relay_copy(index, by, 0).start()

    def serve_cross(index):
        for by in range(1, chips):
            for step in range(1, groups):
                cross_arrival(index, by, step).wait_recv()
                relay_copy(index, by, step).start()

    def weights_ready(layer, m):
        index = layer * 4 + m
        own_copy(layer, m).wait()
        pair_copy(layer, m, partner).wait_recv()
        for by in range(1, chips):
            for step in range(groups):
                relay_copy(index, by, step, True).wait_recv()

    def columns(owner):
        return pl.ds(pl.multiple_of(owner * width, 128), width)

    def act_copy(c, stage, owner, to, send):
        ref = gathers[c].at[stage, :, columns(owner)]
        return remote(ref, ref, send, act_recv.at[c, stage, owner], {"tp": to})

    OFFSETS = (2, -2, 1, -1)

    def inside(index):
        return (index >= 0) & (index < tp_count)

    def act_each(c, stage, what):
        for j, by in enumerate(OFFSETS):
            if abs(by) < tp_count:

                @pl.when(inside(t + by))
                def _(j=j, by=by):
                    what(act_copy(c, stage, t, t + by, act_send.at[c, stage, j]))

    def act_forwards(c, stage, start):
        for k in range(1, (tp_count + 1) // 2):
            for side, sign in enumerate((1, -1)):
                origin = t - 2 * k * sign

                @pl.when(inside(origin) & inside(t + sign))
                def _(k=k, side=side, sign=sign, origin=origin):
                    if start:
                        act_copy(c, stage, origin, t + sign, act_fwd.at[c, stage, k - 1, side, 0]).wait_recv()
                    for far in (2, 1):

                        @pl.when(inside(t + sign * far))
                        def _(far=far):
                            copy = act_copy(
                                c, stage, origin, t + sign * far, act_fwd.at[c, stage, k - 1, side, far - 1]
                            )
                            if start:
                                copy.start()
                            else:
                                copy.wait_send()

    def act_finish(c, stage):
        for owner in range(tp_count):
            right = (owner < t) & (lax.rem(t - owner + tp_count * 2, 2) == 0) & (t + 1 < tp_count)
            left = (owner > t) & (lax.rem(owner - t + tp_count * 2, 2) == 0) & (t >= 1)

            @pl.when((owner != t) & jnp.logical_not(right | left))
            def _(owner=owner):
                act_copy(c, stage, owner, t, act_send.at[c, stage, 0]).wait_recv()

    def sq_copy(c, index, by):
        ref = squares[c].at[index, t]
        return remote(
            ref,
            ref,
            sq_send.at[c, index, by - 1],
            sq_recv.at[c, index, by - 1],
            {"tp": lax.rem(t + by, tp_count)},
        )

    def span(c):
        return pl.ds(starts[c], counts[c])

    def send_normed(c, layer):
        now = stream[span(c), :]
        gathers[c][2 * layer, :, columns(t)] = (now * gains[pl.ds(layer, 1), :]).astype(jnp.bfloat16)
        act_each(c, 2 * layer, lambda copy: copy.start())

    def send_squares(c, index):
        now = stream[span(c), :]
        sums = lax.dot_general(
            jnp.ones((8, width), jnp.float32),
            now * now,
            (((1,), (1,)), ((), ())),
            precision=lax.Precision.HIGHEST,
            preferred_element_type=jnp.float32,
        )
        squares[c][index, t, :, 0 : counts[c]] = sums
        for by in range(1, tp_count):
            sq_copy(c, index, by).start()

    def row_scale(c, index):
        for by in range(1, tp_count):
            sq_copy(c, index, by).wait_recv()
        total = squares[c][index, 0]
        for owner in range(1, tp_count):
            total = total + squares[c][index, owner]
        scale = lax.rsqrt(total / full + epsilon)
        return jnp.transpose(scale)[0 : counts[c], 0:1]

    @pl.when(s + 1 < sp_count)
    def _():
        remote(
            tokens.at[pl.ds(rows - HALO, HALO), :], halo, halo_sems.at[0], halo_sems.at[1], {"sp": s + 1}
        ).start()

    for layer in range(1):
        for m in range(3):
            for by in range(1, chips):
                row_copy(layer, m, by).start()
            pair_copy(layer, m, s).start()
            own_copy(layer, m).start()

    stream[HALO:, :] = tokens[...].astype(jnp.float32)
    send_normed(1, 0)

    @pl.when(s > 0)
    def _():
        remote(halo, halo, halo_sems.at[0], halo_sems.at[1], {"sp": partner}).wait_recv()

    stream[0:HALO, :] = halo[...].astype(jnp.float32)
    send_normed(0, 0)
    send_squares(0, 0)
    send_squares(1, 0)

    for index in range(3, layers * 4):
        layer, m = divmod(index, 4)
        for by in range(1, chips):
            row_copy(layer, m, by).start()
        pair_copy(layer, m, s).start()
        own_copy(layer, m).start()

    act_forwards(0, 0, True)
    act_forwards(1, 0, True)
    serve_rows(0)
    serve_rows(1)
    serve_cross(0)
    serve_rows(2)
    serve_cross(1)

    def project(c, layer):
        stage = 2 * layer
        act_finish(c, stage)
        if c == 0:
            for m in range(3):
                weights_ready(layer, m)
        seen = gathers[c][stage]
        scale = row_scale(c, layer)
        ins, values, outs = [
            (jnp.dot(seen, weights[layer * 4 + m], preferred_element_type=jnp.float32) * scale).astype(jnp.bfloat16)
            for m in range(3)
        ]
        made = (ins.astype(jnp.float32) * values.astype(jnp.float32)).astype(jnp.bfloat16)
        products[pl.ds(8 + starts[c], counts[c]), :] = made.astype(jnp.float32)
        total = None
        for k in range(tap_count):
            term = products[pl.ds(8 + starts[c] - (tap_count - 1) + k, counts[c]), :] * taps[layer, pl.ds(k, 1), :]
            total = term if total is None else total + term
        gathers[c][stage + 1, :, columns(t)] = (outs.astype(jnp.float32) * total).astype(jnp.bfloat16)
        act_each(c, stage + 1, lambda copy: copy.start())

    def mix(c, layer):
        stage = 2 * layer + 1
        act_finish(c, stage)
        if c == 0:
            weights_ready(layer, 3)
        stream[span(c), :] += jnp.dot(
            gathers[c][stage], weights[layer * 4 + 3], preferred_element_type=jnp.float32
        )

        @pl.when(layer + 1 < layers)
        def _():
            send_normed(c, layer + 1)

        send_squares(c, layer + 1)

    def one_layer(layer, carry):
        index = 4 * layer
        more = layer + 1 < layers

        @pl.when(layer > 0)
        def _():
            act_forwards(0, 2 * layer, True)

        serve_cross(index + 2)
        project(0, layer)

        @pl.when(layer > 0)
        def _():
            act_forwards(1, 2 * layer, True)

        project(1, layer)
        serve_rows(index + 3)
        act_forwards(0, 2 * layer + 1, True)
        serve_cross(index + 3)
        mix(0, layer)
        act_forwards(1, 2 * layer + 1, True)

        @pl.when(more)
        def _():
            serve_rows(index + 4)
            serve_rows(index + 5)
            serve_cross(index + 4)

        mix(1, layer)

        @pl.when(more)
        def _():
            serve_rows(index + 6)
            serve_cross(index + 5)

        return carry

    lax.fori_loop(0, layers, one_layer, 0)

    for c in range(2):
        first = HALO if c == 0 else 0
        scale = row_scale(c, layers)[first:]
        now = stream[pl.ds(starts[c] + first, counts[c] - first), :]
        done = (now * scale * final_gain[...]).astype(jnp.bfloat16)
        out[pl.ds(starts[c] + first - HALO, counts[c] - first), :] = done

    @pl.when(s + 1 < sp_count)
    def _():
        remote(
            tokens.at[pl.ds(rows - HALO, HALO), :], halo, halo_sems.at[0], halo_sems.at[1], {"sp": s + 1}
        ).wait_send()

    def drain_weights(index, carry):
        layer = index // 4
        pair = remote(
            mats[0].at[layer], whole_block(index, s), pair_send.at[index], pair_recv.at[index], {"sp": partner}
        )
        pair.wait_send()
        for by in range(1, chips):
            row_arrival(index, by).wait_send()
            for step in range(1, groups):
                cross_copy(index, by, step).wait_send()
            for step in range(groups):
                relay_copy(index, by, step).wait_send()
        return carry

    lax.fori_loop(0, layers * 4, drain_weights, 0)

    def drain_acts(stage, carry):
        for c in range(2):
            act_each(c, stage, lambda copy: copy.wait_send())
            act_forwards(c, stage, False)
        return carry

    lax.fori_loop(0, layers * 2, drain_acts, 0)

    def drain_squares(index, carry):
        for c in range(2):
            for by in range(1, tp_count):
                sq_copy(c, index, by).wait_send()
        return carry

    lax.fori_loop(0, layers + 1, drain_squares, 0)


def shards(sizes, tokens_in, out_gate, in_gate, value_proj, mix_proj, conv_taps, norm_gains, final_gain):
    groups, sp_count, tp_count, layers, tap_count = sizes
    rows, width = tokens_in.shape
    full = width * tp_count
    chips = sp_count // CORES
    half = rows // 2
    first, second = HALO + half, rows - half
    lanes = lambda n: -(-n // 128) * 128
    dma = pltpu.SemaphoreType.DMA
    near, rounds = max(chips - 1, 1), max((tp_count + 1) // 2 - 1, 1)
    mats = layers * 4
    vmem = pl.BlockSpec(memory_space=pltpu.VMEM)
    hbm = pl.BlockSpec(memory_space=pl.ANY)
    return pl.pallas_call(
        functools.partial(kernel, sizes),
        out_shape=jax.ShapeDtypeStruct((rows, width), jnp.bfloat16),
        in_specs=[vmem] + [hbm] * 4 + [vmem] * 3,
        out_specs=vmem,
        scratch_shapes=[
            pltpu.VMEM((mats, full, width), jnp.bfloat16),
            pltpu.VMEM((2 * layers, first, full), jnp.bfloat16),
            pltpu.VMEM((2 * layers, second, full), jnp.bfloat16),
            pltpu.VMEM((layers + 1, tp_count, 8, lanes(first)), jnp.float32),
            pltpu.VMEM((layers + 1, tp_count, 8, lanes(second)), jnp.float32),
            pltpu.VMEM((HALO + rows, width), jnp.float32),
            pltpu.VMEM((8 + HALO + rows, width), jnp.float32),
            pltpu.VMEM((HALO, width), jnp.bfloat16),
            dma((mats,)),
            dma((2,)),
            dma((mats,)),
            dma((mats,)),
            dma((mats, near)),
            dma((mats, near)),
            dma((mats, near, max(groups - 1, 1))),
            dma((mats, near, max(groups - 1, 1))),
            dma((mats, near, groups)),
            dma((mats, near, groups)),
            dma((2, 2 * layers, 4)),
            dma((2, 2 * layers, tp_count)),
            dma((2, 2 * layers, rounds, 2, 2)),
            dma((2, layers + 1, max(tp_count - 1, 1))),
            dma((2, layers + 1, max(tp_count - 1, 1))),
        ],
        compiler_params=pltpu.CompilerParams(
            collective_id=0, has_side_effects=True, vmem_limit_bytes=VMEM_LIMIT
        ),
    )(tokens_in, in_gate, value_proj, out_gate, mix_proj, conv_taps, norm_gains, final_gain.reshape(1, width))


def solution(mesh):
    in_specs = (
        P(("grp", "sp"), "tp"),
        P(None, "sp", "tp"),
        P(None, "sp", "tp"),
        P(None, "sp", "tp"),
        P(None, "sp", "tp"),
        P(None, None, "tp"),
        P(None, "tp"),
        P("tp"),
    )
    out_specs = P(("grp", "sp"), "tp")

    def body(*args):
        taps = args[5]
        sizes = (mesh.shape["grp"], mesh.shape["sp"], mesh.shape["tp"], taps.shape[0], taps.shape[1])
        return shards(sizes, *args)

    return jax.shard_map(body, mesh=mesh, in_specs=in_specs, out_specs=out_specs, check_vma=False)
```

time: 425 us -> 142 us (0.33)
  waiting for transfers between devices: 323 us -> 0 us
  Pallas kernels: 0 us -> 140 us
  blocking collectives: 44.2 us -> 0 us
  matrix products: 34.6 us -> 0 us
  between operations: 13.7 us -> 0.01 us
  starting transfers between devices: 5.1 us -> 0 us
    all_gather x10 -> x0, waiting for transfers between devices: 319 us -> none  [the longest x3 90 us: shards(): spread = lax.all_gather(gated, 'tp', axis=1, tiled=True)]
    pallas_call x0 -> x1, Pallas kernels: none -> 140 us  [shards(): pl.pallas_call(functools.partial(kernel, sizes), out_shape=jax.ShapeDtype...]
    psum x4 -> x0, blocking collectives: 44.2 us -> none  [row_scale(): squares = lax.psum(jnp.sum(stream * stream, axis=1, keepdims=True), 'tp')]
    dot_general x12 -> x0, matrix products: 34.6 us -> none  [the longest x9 25.2 us: shards(): jnp.dot(gathered, weight[layer_index], preferred_element_type=jnp.float32)]
    ppermute x3 -> x0, starting transfers between devices: 4.73 us -> none  [passed_along(): return lax.ppermute(shard, axis, pairs)]
  transfers between devices with their start and end apart: 13 -> 0, of which waited for: 12 -> 0; matrix products, arithmetic and copies ran while one was open for 2% -> 0% of each run, Pallas kernels for 0% -> 0%
where the time goes in v1:
time: 142 us
  Pallas kernels  140 us (99%)
  local copies, waits for them, and re-layouts  1.67 us (1%)
    pallas_call x1, Pallas kernels, shards(): pl.pallas_call(functools.partial(kernel, sizes), out_shape=jax.ShapeDtype...  140 us

profile of v1, /device:TPU:0, one launch (start us, length us, event | category | flops | bytes accessed | tf_op | source)
XLA Modules:
  0.0 142.1 jit_solution(15696029074262784710)
XLA Ops:
  0.0 140.4 %shard_map.82 = bf16[256,512]{1,0:T(8,128)(2,1)} custom-call(bf16[256,512]{1,0:T(8,128)(2,1)} %tokens.1, bf16[3,512,512]{2,1,0:T(8,128)(2,1)} %in_gate.1, bf16[3,512,512]{2,1,0:T(8,128)(2,1)} %value_proj.1, bf16[3,512,512]{2,1,0:T(8,128)(2,1)} %out_gate.1, bf16[3,512,512]{2,1,0:T(8,128)(2,1)} %mix_proj.1, f32[3,3,512]{2,1,0:T(4,128)} %taps.1, ...), custom_call_target="tpu_custom_call" | custom-call | tf_op jit(solution)/shard_map/pallas_call | solution.py:439
  140.4 1.7 %copy.10 = bf16[256,512]{1,0:T(8,128)(2,1)} copy(bf16[256,512]{1,0:T(8,128)(2,1)} %shard_map.82) | data formatting | bytes 524288

commit v2 on v1

--- a/solution.py
+++ b/solution.py
@@ -9,7 +9,7 @@
 
 epsilon = 1e-06
 MESH = pl.DeviceIdType.MESH
-HALO = 16
+HALO = 8
 CORES = 2
 VMEM_LIMIT = 67043328
 
@@ -302,18 +302,21 @@
     serve_rows(2)
     serve_cross(1)
 
-    def project(c, layer):
+    def project(c, layer, before):
         stage = 2 * layer
         act_finish(c, stage)
-        if c == 0:
-            for m in range(3):
-                weights_ready(layer, m)
         seen = gathers[c][stage]
         scale = row_scale(c, layer)
-        ins, values, outs = [
-            (jnp.dot(seen, weights[layer * 4 + m], preferred_element_type=jnp.float32) * scale).astype(jnp.bfloat16)
-            for m in range(3)
-        ]
+
+        def projected(m):
+            if c == 0:
+                if m == 2:
+                    pl.when(layer == 0)(lambda: serve_cross(2))
+                weights_ready(layer, m)
+            product = jnp.dot(seen, weights[layer * 4 + m], preferred_element_type=jnp.float32)
+            return (product * scale).astype(jnp.bfloat16)
+
+        ins, values, outs = [projected(m) for m in range(3)]
         made = (ins.astype(jnp.float32) * values.astype(jnp.float32)).astype(jnp.bfloat16)
         products[pl.ds(8 + starts[c], counts[c]), :] = made.astype(jnp.float32)
         total = None
@@ -321,9 +324,10 @@
             term = products[pl.ds(8 + starts[c] - (tap_count - 1) + k, counts[c]), :] * taps[layer, pl.ds(k, 1), :]
             total = term if total is None else total + term
         gathers[c][stage + 1, :, columns(t)] = (outs.astype(jnp.float32) * total).astype(jnp.bfloat16)
+        before()
         act_each(c, stage + 1, lambda copy: copy.start())
 
-    def mix(c, layer):
+    def mix(c, layer, before):
         stage = 2 * layer + 1
         act_finish(c, stage)
         if c == 0:
@@ -332,6 +336,8 @@
             gathers[c][stage], weights[layer * 4 + 3], preferred_element_type=jnp.float32
         )
 
+        before()
+
         @pl.when(layer + 1 < layers)
         def _():
             send_normed(c, layer + 1)
@@ -342,37 +348,38 @@
         index = 4 * layer
         more = layer + 1 < layers
 
-        @pl.when(layer > 0)
-        def _():
-            act_forwards(0, 2 * layer, True)
-
-        serve_cross(index + 2)
-        project(0, layer)
-
-        @pl.when(layer > 0)
-        def _():
-            act_forwards(1, 2 * layer, True)
-
-        project(1, layer)
-        serve_rows(index + 3)
-        act_forwards(0, 2 * layer + 1, True)
-        serve_cross(index + 3)
-        mix(0, layer)
-        act_forwards(1, 2 * layer + 1, True)
-
-        @pl.when(more)
-        def _():
-            serve_rows(index + 4)
-            serve_rows(index + 5)
-            serve_cross(index + 4)
-
-        mix(1, layer)
-
-        @pl.when(more)
-        def _():
-            serve_rows(index + 6)
-            serve_cross(index + 5)
-
+        def pass_first():
+            @pl.when(more)
+            def _():
+                act_forwards(0, 2 * layer + 2, True)
+
+        def pass_second():
+            @pl.when(layer > 0)
+            def _():
+                act_forwards(1, 2 * layer, True)
+
+        def serve(first, row_ahead, cross_ahead):
+            @pl.when(layer == 0)
+            def _():
+                for action, at in first:
+                    action(at)
+
+            @pl.when((layer > 0) & (index + row_ahead < layers * 4))
+            def _():
+                serve_rows(index + row_ahead)
+
+            @pl.when((layer > 0) & (index + cross_ahead < layers * 4))
+            def _():
+                serve_cross(index + cross_ahead)
+
+        project(0, layer, pass_second)
+        serve(((serve_rows, 3), (serve_rows, 4)), 5, 3)
+        project(1, layer, lambda: act_forwards(0, 2 * layer + 1, True))
+        serve(((serve_rows, 5), (serve_cross, 3)), 6, 4)
+        mix(0, layer, lambda: act_forwards(1, 2 * layer + 1, True))
+        serve(((serve_rows, 6), (serve_cross, 4)), 7, 5)
+        mix(1, layer, pass_first)
+        serve(((serve_rows, 7), (serve_cross, 5), (serve_rows, 8), (serve_cross, 6)), 8, 6)
         return carry
 
     lax.fori_loop(0, layers, one_layer, 0)

time: 142 us -> 137 us (0.965)
  Pallas kernels: 140 us -> 135 us
    pallas_call x1, Pallas kernels: 140 us -> 135 us  [shards(): pl.pallas_call(functools.partial(kernel, sizes), out_shape=jax.ShapeDtype...]
where the time goes in v2:
time: 137 us
  Pallas kernels  135 us (99%)
  local copies, waits for them, and re-layouts  1.67 us (1%)
    pallas_call x1, Pallas kernels, shards(): pl.pallas_call(functools.partial(kernel, sizes), out_shape=jax.ShapeDtype...  135 us

profile of v2, /device:TPU:0, one launch (start us, length us, event | category | flops | bytes accessed | tf_op | source)
XLA Modules:
  0.0 136.9 jit_solution(7195533316599586989)
XLA Ops:
  0.0 135.3 %shard_map.82 = bf16[256,512]{1,0:T(8,128)(2,1)} custom-call(bf16[256,512]{1,0:T(8,128)(2,1)} %tokens.1, bf16[3,512,512]{2,1,0:T(8,128)(2,1)} %in_gate.1, bf16[3,512,512]{2,1,0:T(8,128)(2,1)} %value_proj.1, bf16[3,512,512]{2,1,0:T(8,128)(2,1)} %out_gate.1, bf16[3,512,512]{2,1,0:T(8,128)(2,1)} %mix_proj.1, f32[3,3,512]{2,1,0:T(4,128)} %taps.1, ...), custom_call_target="tpu_custom_call" | custom-call | tf_op jit(solution)/shard_map/pallas_call | solution.py:446
  135.3 1.7 %copy.10 = bf16[256,512]{1,0:T(8,128)(2,1)} copy(bf16[256,512]{1,0:T(8,128)(2,1)} %shard_map.82) | data formatting | bytes 524288
